TPU v7x, 32 devices: a whole 2x2x4 slice. The times are simulated.
32 devices in a mesh: ra: 8 (over z, y), cb: 4 (over x, core).
Axes of the slice: x: 2, y: 2, z: 4, core: 2. Of those that a mesh axis runs over, the one named last changes fastest.
Arguments:
- tokens: bfloat16 [1024, 4096], P(None, 'ra'), may hold values from -40 to 40
- norm_gain: float32 [4096], P('ra'), may hold values from 0.1 to 1.9
- gate_weight: bfloat16 [4096, 11264], P('ra', 'cb'), may hold values from -0.09375 to 0.09375
- up_weight: bfloat16 [4096, 11264], P('ra', 'cb'), may hold values from -0.09375 to 0.09375
- down_weight: bfloat16 [11264, 4096], P('cb', 'ra'), may hold values from -0.0546875 to 0.0546875
- out_gain: float32 [4096], P('ra'), may hold values from 0.1 to 1.9
Outputs:
- normed: bfloat16 [1024, 4096], P(None, 'ra')
All inputs are finite; a program needn't handle non-finite values.
Results may differ from a plain program's by a relative error of at most 0.0076.
Values may be sent and summed in bfloat16 or wider, within the bound.
No kernel may reach another device: no remote copies, remote signals or barrier semaphores. Data moves between devices by JAX's collectives and lax.ppermute only.
A program may use at most 128 MiB of HBM per device.

v0:
```python
import jax
import jax.numpy as jnp
from jax import lax
from jax.sharding import PartitionSpec as P

D = 4096


def body(tokens, norm_gain, gate_weight, up_weight, down_weight, out_gain):
    stream_in = tokens.astype(jnp.float32)
    local_sq = jnp.sum(stream_in * stream_in, axis=1)
    scaled = (stream_in * norm_gain[None, :]).astype(jnp.bfloat16)
    gate_part = jnp.dot(scaled, gate_weight, preferred_element_type=jnp.float32)
    up_part = jnp.dot(scaled, up_weight, preferred_element_type=jnp.float32)
    gate_sum, up_sum, sq_sum = (
        lax.psum_scatter(gate_part, "ra", scatter_dimension=0, tiled=True),
        lax.psum_scatter(up_part, "ra", scatter_dimension=0, tiled=True),
        lax.psum_scatter(local_sq, "ra", scatter_dimension=0, tiled=True),
    )
    inv_rms = jax.lax.rsqrt(sq_sum / D + 1e-06)[:, None]
    hidden = (jax.nn.silu(gate_sum * inv_rms) * (up_sum * inv_rms)).astype(jnp.bfloat16)
    down_part = jnp.dot(
        lax.all_gather(hidden, "ra", axis=0, tiled=True),
        down_weight,
        preferred_element_type=jnp.float32,
    )
    branch = lax.psum(down_part, "cb")
    stream = 0.5 * stream_in + branch
    total_sq = lax.psum(jnp.sum(stream * stream, axis=1), "ra")
    factor = jax.lax.rsqrt(total_sq / D + 1e-06)[:, None]
    return (stream * factor * out_gain[None, :]).astype(jnp.bfloat16)


def solution(mesh):
    placed = (P(None, "ra"), P("ra"), P("ra", "cb"), P("ra", "cb"), P("cb", "ra"), P("ra"))
    return jax.shard_map(body, mesh=mesh, in_specs=placed, out_specs=P(None, "ra"), check_vma=False)
```

profile of v0, /device:TPU:0, one launch (start us, length us, event | category | flops | bytes accessed | tf_op | source)
XLA Modules:
  0.0 593.5 jit_solution(14529803967618089035)
XLA Ops:
  6.5 0.0 copy-start
  6.5 0.0 reduce-scatter.3.cloned.1.call-start
  6.5 1.8 copy-done
  8.4 7.5 %fusion.5 = f32[1024,2816]{1,0:T(8,128)} fusion(bf16[512,2816]{1,0:T(8,128)(2,1)S(1)} %copy-done, bf16[1024,512]{1,0:T(8,128)(2,1)} %param.6, f32[512]{0:T(512)} %param.7), kind=kOutput, calls=%fused_computation.10 | convolution fusion | flops 2954362880 | bytes 15468544 | tf_op jit(solution)/shard_map/dot_general | solution.py:13
  15.8 0.0 copy-start.2
  15.8 0.0 reduce-scatter.3.cloned.1.call-update
  15.9 0.0 reduce-scatter.5.cloned.1.call-start
  15.9 0.6 copy-done.2
  16.5 9.9 %fusion.3 = f32[1024,2816]{1,0:T(8,128)} fusion(bf16[512,2816]{1,0:T(8,128)(2,1)} %param.9, bf16[1024,512]{1,0:T(8,128)(2,1)} %param.6, f32[512]{0:T(512)S(1)} %copy-done.2), kind=kOutput, calls=%fused_computation.9 | convolution fusion | flops 2954362880 | bytes 15468544 | tf_op jit(solution)/shard_map/dot_general | solution.py:14
  26.4 0.0 copy-start.3
  26.4 0.0 reduce-scatter.5.cloned.1.call-update
  26.4 0.0 all-gather.2.cloned.1.call-start
  26.5 0.6 copy-done.3
  27.0 0.6 dynamic-slice
  28.3 1.5 fusion.2
  29.8 24.5 %all-reduce = f32[1024]{0:T(1024)S(1)} all-reduce(f32[1024]{0:T(1024)S(1)} %fusion.2), channel_id=3, replica_groups=mesh['ra'=8,'cb'=4] {'ra'}, use_global_device_ids=true, to_apply=%region_2.0.clone | all-reduce | flops 1024 | bytes 8192
  54.3 0.1 fusion.8
  54.4 157.7 %reduce-scatter.3.cloned.1.call-done = f32[128,2816]{1,0:T(8,128)} async-done(((f32[1024,2816]{1,0:T(8,128)}), f32[128,2816]{1,0:T(8,128)}) %reduce-scatter.3.cloned.1.call-update) | async-done | bytes 1441808 | tf_op jit(solution)/shard_map/reduce_scatter | solution.py:16
  212.1 195.6 %reduce-scatter.5.cloned.1.call-done = f32[128,2816]{1,0:T(8,128)} async-done(((f32[1024,2816]{1,0:T(8,128)}), f32[128,2816]{1,0:T(8,128)}) %reduce-scatter.5.cloned.1.call-update) | async-done | bytes 1441808 | tf_op jit(solution)/shard_map/reduce_scatter | solution.py:17
  407.7 3.1 multiply_convert_fusion.1
  410.8 0.0 all-gather.2.cloned.1.call-update
  410.8 0.0 all-reduce.3.cloned.1.call-start
  410.9 91.5 %all-gather.2.cloned.1.call-done = bf16[1024,2816]{1,0:T(8,128)(2,1)} async-done(((bf16[128,2816]{1,0:T(8,128)(2,1)}), bf16[1024,2816]{1,0:T(8,128)(2,1)}) %all-gather.2.cloned.1.call-update) | async-done | bytes 5767184 | tf_op jit(solution)/shard_map/all_gather | solution.py:23
  502.4 8.0 %fusion.9 = f32[1024,512]{1,0:T(8,128)} fusion(bf16[1024,2816]{1,0:T(8,128)(2,1)} %all-gather.2.cloned.1.call-done, bf16[2816,512]{1,0:T(8,128)(2,1)} %param.10), kind=kOutput, calls=%fused_computation.15 | convolution fusion | flops 2952790016 | bytes 10747904 | tf_op jit(solution)/shard_map/dot_general | solution.py:22
  510.4 0.0 all-reduce.3.cloned.1.call-update
  510.4 0.0 copy-start.1
  510.4 49.7 %all-reduce.3.cloned.1.call-done = f32[1024,512]{1,0:T(8,128)} async-done(((f32[1024,512]{1,0:T(8,128)}), f32[1024,512]{1,0:T(8,128)}) %all-reduce.3.cloned.1.call-update) | async-done | bytes 2097168 | tf_op jit(solution)/shard_map/psum | solution.py:27
  560.1 2.3 multiply_reduce_fusion
  562.4 21.4 %psum.15 = f32[1024]{0:T(1024)S(1)} all-reduce(f32[1024]{0:T(1024)S(1)} %multiply_reduce_fusion), channel_id=1, replica_groups=mesh['ra'=8,'cb'=4] {'ra'}, use_global_device_ids=true, to_apply=%region_6.7 | all-reduce | flops 1024 | bytes 8192 | tf_op jit(solution)/shard_map/psum | solution.py:29
  583.7 0.0 copy-done.1
  583.7 3.2 multiply_convert_fusion
  (1 shorter events, 0.0 us)
Async XLA Ops:
  6.5 1.8 copy-start
  6.5 205.6 %reduce-scatter.3.cloned.1.call-start = ((), (), s32[]{:S(2)}) async-start(), calls=%async_computation.2 | async-start | bytes 12976128 | tf_op jit(solution)/shard_map/reduce_scatter | solution.py:16
  15.8 0.7 copy-start.2
  15.9 391.8 %reduce-scatter.5.cloned.1.call-start = ((), (), s32[]{:S(2)}) async-start(), calls=%async_computation.3 | async-start | bytes 12976128 | tf_op jit(solution)/shard_map/reduce_scatter | solution.py:17
  26.4 0.7 copy-start.3
  26.4 476.0 %all-gather.2.cloned.1.call-start = ((), (), s32[]{:S(2)}) async-start(), calls=%async_computation.4 | async-start | bytes 6488064 | tf_op jit(solution)/shard_map/all_gather | solution.py:23
  410.8 149.3 %all-reduce.3.cloned.1.call-start = ((), (), s32[]{:S(2)}) async-start(), calls=%async_computation.5 | async-start | bytes 4194304 | tf_op jit(solution)/shard_map/psum | solution.py:27
  510.4 73.4 %copy-start.1 = (f32[512]{0:T(512)S(1)}, f32[512]{0:T(512)}, u32[]{:S(2)}) copy-start(f32[512]{0:T(512)} %param.11) | copy-start | bytes 6148
Sparse Core Ops, SparseCore 0:
  16.0 196.0 reduce-scatter.2
  215.7 191.9 reduce-scatter.4
  410.9 91.4 all-gather.1
  510.5 49.5 all-reduce.2
where the time goes:
time: 594 us; the launch traced here: 593 us
  waiting for transfers between devices  495 us (83%)
  blocking collectives  45.9 us (8%)
  matrix products  25.3 us (4%)
  between operations  13.8 us (2%)
  other arithmetic  10.2 us (2%)
    reduce_scatter x1, waiting for transfers between devices, body(): lax.psum_scatter(up_part, 'ra', scatter_dimension=0, tiled=True)  196 us
    reduce_scatter x1, waiting for transfers between devices, body(): lax.psum_scatter(gate_part, 'ra', scatter_dimension=0, tiled=True)  158 us
    all_gather x1, waiting for transfers between devices, body(): lax.all_gather(hidden, 'ra', axis=0, tiled=True)  91.5 us
    psum x1, waiting for transfers between devices, body(): branch = lax.psum(down_part, 'cb')  49.7 us
    unnamed x1, blocking collectives  24.5 us
    psum x1, blocking collectives, body(): total_sq = lax.psum(jnp.sum(stream * stream, axis=1), 'ra')  21.4 us
  transfers between devices with their start and end apart: 4, of which 4 were waited for; matrix products, arithmetic and copies ran while one was open for 2% of the time, Pallas kernels for 0%

commit v1 on v0

--- a/solution.py
+++ b/solution.py
@@ -24,7 +24,9 @@
         down_weight,
         preferred_element_type=jnp.float32,
     )
-    branch = lax.psum(down_part, "cb")
+    branch = down_part
+    for hop in (1, 2):
+        branch = branch + lax.ppermute(branch, "cb", [(dev, dev ^ hop) for dev in range(4)])
     stream = 0.5 * stream_in + branch
     total_sq = lax.psum(jnp.sum(stream * stream, axis=1), "ra")
     factor = jax.lax.rsqrt(total_sq / D + 1e-06)[:, None]

time: 594 us -> 595 us (level)
    ppermute x0 -> x2, waiting for transfers between devices: none -> 50.3 us  [body(): lax.ppermute(branch, 'cb', [(dev, dev ^ hop) for dev in range(4)])]
    psum x1 -> x0, waiting for transfers between devices: 49.7 us -> none  [body(): branch = lax.psum(down_part, 'cb')]
  transfers between devices with their start and end apart: 4 -> 5, of which waited for: 4 -> 5; matrix products, arithmetic and copies ran while one was open for 2% -> 2% of each run, Pallas kernels for 0% -> 0%
where the time goes in v1:
time: 595 us
  waiting for transfers between devices  495 us (83%)
  blocking collectives  43.5 us (7%)
  matrix products  23.5 us (4%)
  between operations  13.7 us (2%)
  other arithmetic  9.61 us (2%)
  local copies, waits for them, and re-layouts  7.19 us (1%)
    reduce_scatter x1, waiting for transfers between devices, body(): lax.psum_scatter(up_part, 'ra', scatter_dimension=0, tiled=True)  196 us
    reduce_scatter x1, waiting for transfers between devices, body(): lax.psum_scatter(gate_part, 'ra', scatter_dimension=0, tiled=True)  158 us
    all_gather x1, waiting for transfers between devices, body(): lax.all_gather(hidden, 'ra', axis=0, tiled=True)  91.6 us
    ppermute x2, waiting for transfers between devices, body(): lax.ppermute(branch, 'cb', [(dev, dev ^ hop) for dev in range(4)])  50.3 us
    unnamed x1, blocking collectives  25 us
    psum x1, blocking collectives, body(): total_sq = lax.psum(jnp.sum(stream * stream, axis=1), 'ra')  18.6 us
  transfers between devices with their start and end apart: 5, of which 5 were waited for; matrix products, arithmetic and copies ran while one was open for 2% of the time, Pallas kernels for 0%

profile of v1, /device:TPU:0, one launch (start us, length us, event | category | flops | bytes accessed | tf_op | source)
XLA Modules:
  0.0 594.7 jit_solution(4166607993195009259)
XLA Ops:
  6.5 2.4 copy.9
  9.0 7.7 %fusion.5 = f32[1024,2816]{1,0:T(8,128)} fusion(bf16[512,2816]{1,0:T(8,128)(2,1)S(1)} %copy-done, bf16[1024,512]{0,1:T(8,128)(2,1)} %copy.9, f32[512]{0:T(512)S(1)} %copy-done.5), kind=kOutput, calls=%fused_computation.10 | convolution fusion | flops 2954362880 | bytes 15468544 | tf_op jit(solution)/shard_map/dot_general | solution.py:13
  16.7 0.0 reduce-scatter.3.cloned.1.call-update
  16.7 0.0 reduce-scatter.5.cloned.1.call-start
  16.8 9.7 %fusion.3 = f32[1024,2816]{1,0:T(8,128)} fusion(bf16[512,2816]{1,0:T(8,128)(2,1)} %param.9, bf16[1024,512]{0,1:T(8,128)(2,1)} %copy.9, f32[512]{0:T(512)S(1)} %copy-done.5), kind=kOutput, calls=%fused_computation.9 | convolution fusion | flops 2954362880 | bytes 15468544 | tf_op jit(solution)/shard_map/dot_general | solution.py:14
  26.4 0.0 reduce-scatter.5.cloned.1.call-update
  26.5 0.0 all-gather.2.cloned.1.call-start
  26.5 0.6 copy-done.6
  27.1 0.6 dynamic-slice
  28.3 1.5 fusion.2
  29.7 25.0 %all-reduce = f32[1024]{0:T(1024)S(1)} all-reduce(f32[1024]{0:T(1024)S(1)} %fusion.2), channel_id=3, replica_groups=mesh['ra'=8,'cb'=4] {'ra'}, use_global_device_ids=true, to_apply=%region_2.0.clone | all-reduce | flops 1024 | bytes 8192
  54.7 0.1 fusion.8
  54.8 157.9 %reduce-scatter.3.cloned.1.call-done = f32[128,2816]{1,0:T(8,128)} async-done(((f32[1024,2816]{1,0:T(8,128)}), f32[128,2816]{1,0:T(8,128)}) %reduce-scatter.3.cloned.1.call-update) | async-done | bytes 1441808 | tf_op jit(solution)/shard_map/reduce_scatter | solution.py:16
  212.7 195.6 %reduce-scatter.5.cloned.1.call-done = f32[128,2816]{1,0:T(8,128)} async-done(((f32[1024,2816]{1,0:T(8,128)}), f32[128,2816]{1,0:T(8,128)}) %reduce-scatter.5.cloned.1.call-update) | async-done | bytes 1441808 | tf_op jit(solution)/shard_map/reduce_scatter | solution.py:17
  408.3 3.1 multiply_convert_fusion.1
  411.4 0.0 all-gather.2.cloned.1.call-update
  411.4 91.6 %all-gather.2.cloned.1.call-done = bf16[1024,2816]{1,0:T(8,128)(2,1)} async-done(((bf16[128,2816]{1,0:T(8,128)(2,1)}), bf16[1024,2816]{1,0:T(8,128)(2,1)}) %all-gather.2.cloned.1.call-update) | async-done | bytes 5767184 | tf_op jit(solution)/shard_map/all_gather | solution.py:23
  503.0 6.1 %fusion.9 = f32[1024,512]{0,1:T(8,128)S(1)} fusion(bf16[1024,2816]{1,0:T(8,128)(2,1)} %all-gather.2.cloned.1.call-done, bf16[2816,512]{1,0:T(8,128)(2,1)} %param.10), kind=kOutput, calls=%fused_computation.15 | convolution fusion | flops 2952790016 | bytes 10747904 | tf_op jit(solution)/shard_map/dot_general | solution.py:22
  509.1 0.0 copy-start.2
  509.1 0.1 collective-permute-start
  509.2 4.1 collective-permute-done
  513.4 0.4 add.36
  513.8 0.0 copy-start.1
  513.8 0.0 copy-start.4
  513.8 1.5 collective-permute-start.1
  515.3 46.2 %collective-permute-done.1 = f32[1024,512]{0,1:T(8,128)S(1)} collective-permute-done((f32[1024,512]{0,1:T(8,128)S(1)}, f32[1024,512]{0,1:T(8,128)S(1)}, u32[]{:S(2)}, u32[]{:S(2)}) %collective-permute-start.1) | collective-permute-done | bytes 2097184 | tf_op jit(solution)/shard_map/ppermute | solution.py:29
  561.5 1.3 copy-done.3
  562.8 0.6 multiply_reduce_fusion
  563.4 18.6 %psum.7 = f32[1024]{0:T(1024)S(1)} all-reduce(f32[1024]{0:T(1024)S(1)} %multiply_reduce_fusion), channel_id=1, replica_groups=mesh['ra'=8,'cb'=4] {'ra'}, use_global_device_ids=true, to_apply=%region_5.6 | all-reduce | flops 1024 | bytes 8192 | tf_op jit(solution)/shard_map/psum | solution.py:31
  582.0 0.0 copy-done.4
  582.0 3.9 multiply_convert_fusion
  585.9 2.3 copy.10
  (10 shorter events, 0.0 us)
Async XLA Ops:
  6.5 2.4 copy-start
  6.5 2.4 copy-start.5
  6.5 206.1 %reduce-scatter.3.cloned.1.call-start = ((), (), s32[]{:S(2)}) async-start(), calls=%async_computation.2 | async-start | bytes 12976128 | tf_op jit(solution)/shard_map/reduce_scatter | solution.py:16
  16.7 391.5 %reduce-scatter.5.cloned.1.call-start = ((), (), s32[]{:S(2)}) async-start(), calls=%async_computation.3 | async-start | bytes 12976128 | tf_op jit(solution)/shard_map/reduce_scatter | solution.py:17
  26.4 0.7 copy-start.6
  26.5 476.5 %all-gather.2.cloned.1.call-start = ((), (), s32[]{:S(2)}) async-start(), calls=%async_computation.4 | async-start | bytes 6488064 | tf_op jit(solution)/shard_map/all_gather | solution.py:23
  509.1 53.7 %copy-start.2 = (bf16[1024,512]{0,1:T(8,128)(2,1)S(1)}, bf16[1024,512]{0,1:T(8,128)(2,1)}, u32[]{:S(2)}) copy-start(bf16[1024,512]{0,1:T(8,128)(2,1)} %copy.9) | copy-start | bytes 3145732
  509.1 4.2 collective-permute-start
  513.8 47.8 %copy-start.1 = (f32[1024,512]{0,1:T(8,128)}, f32[1024,512]{0,1:T(8,128)S(1)}, u32[]{:S(2)}) copy-start(f32[1024,512]{0,1:T(8,128)S(1)} %add.36) | copy-start | bytes 6291460
  513.8 68.2 %copy-start.4 = (f32[512]{0:T(512)S(1)}, f32[512]{0:T(512)}, u32[]{:S(2)}) copy-start(f32[512]{0:T(512)} %param.11) | copy-start | bytes 6148
  513.8 47.7 %collective-permute-start.1 = (f32[1024,512]{0,1:T(8,128)S(1)}, f32[1024,512]{0,1:T(8,128)S(1)}, u32[]{:S(2)}, u32[]{:S(2)}) collective-permute-start(f32[1024,512]{0,1:T(8,128)S(1)} %add.36), channel_id=1, source_target_pairs={{0,2},{1,3},{2,0},{3,1},{4,6},{5,7},{6,4},{7,5},{8,10},{9,11},{10,... | collective-permute-start | bytes 6291464 | tf_op jit(solution)/shard_map/ppermute | solution.py:29
  561.5 1.3 copy-start.3
Sparse Core Ops, SparseCore 0:
  16.9 195.7 reduce-scatter.2
  216.3 191.9 reduce-scatter.4
  411.5 91.4 all-gather.1
